TPU v7x, 32 devices: a whole 2x2x4 slice. The times are simulated.
32 devices in a mesh: sp: 8 (over z, x), tp: 4 (over y, core).
Axes of the slice: x: 2, y: 2, z: 4, core: 2. Of those that a mesh axis runs over, the one named last changes fastest.
Arguments:
- stream: bfloat16 [2048, 2048], P(('sp', 'tp')), may hold values from -6 to 6
- query_a: bfloat16 [2048, 384], P('sp', 'tp'), may hold values from -400 to 400
- query_b: bfloat16 [2048, 640], P('sp', 'tp'), may hold values from -400 to 400
- latent: bfloat16 [2048, 256], P('sp'), may hold values from -6 to 6
- rotary_key: bfloat16 [2048, 32], P('sp'), may hold values from -6 to 6
- latent_gain: float32 [256], replicated, may hold values from 0.1 to 1.9
- key_gain_a: float32 [96], replicated, may hold values from 0.1 to 1.9
- key_gain_b: float32 [160], replicated, may hold values from 0.1 to 1.9
- w_key_a: bfloat16 [256, 256], P(None, 'tp'), may hold values from -0.375 to 0.375
- w_value_a: bfloat16 [256, 256], P(None, 'tp'), may hold values from -0.375 to 0.375
- w_key_b: bfloat16 [256, 512], P(None, 'tp'), may hold values from -0.375 to 0.375
- w_value_b: bfloat16 [256, 512], P(None, 'tp'), may hold values from -0.375 to 0.375
- w_out_a: bfloat16 [256, 2048], P('tp'), may hold values from -0.21875 to 0.21875
- w_out_b: bfloat16 [512, 2048], P('tp'), may hold values from -0.21875 to 0.21875
- norm_gain: float32 [2048], replicated, may hold values from 0.1 to 1.9
- w_up: bfloat16 [2048, 4096], P('sp', 'tp'), may hold values from -0.125 to 0.125
- w_down: bfloat16 [4096, 2048], P('tp', 'sp'), may hold values from -0.09375 to 0.09375
Outputs:
- result: bfloat16 [2048, 2048], P(('sp', 'tp'))
All inputs are finite; a program needn't handle non-finite values.
Results may differ from a plain program's by a relative error of at most 0.018.
The roundings to bfloat16 on the way count: a program that leaves them out, or rounds other values in their place, can miss the bound.
Values may be sent and summed in bfloat16 or wider, within the bound.
A program may use at most 128 MiB of HBM per device.

v0:
```python
import math

import jax
import jax.numpy as jnp
from jax import lax
from jax.sharding import PartitionSpec as P

NOPE_A = 64
V_A = 64
NOPE_B = 128
V_B = 128
ROPE = 32


EPSILON = 1e-06
THETA = 10000.0


def rms_scale(values, gain):
    wide = values.astype(jnp.float32)
    return wide * lax.rsqrt(jnp.mean(wide * wide, axis=-1, keepdims=True) + EPSILON) * gain


def rotate(tail, positions):
    half = tail.shape[-1] // 2
    freqs = THETA ** (-jnp.arange(half, dtype=jnp.float32) / half)
    angle = positions[:, None, None] * freqs
    cosine = jnp.cos(angle)
    sine = jnp.sin(angle)
    first = tail[..., :half]
    second = tail[..., half:]
    return jnp.concatenate(
        [first * cosine - second * sine, second * cosine + first * sine], axis=-1
    )


def make_keys(normed, rotary_key, w_key, w_value, key_gain, nope, positions):
    count = normed.shape[0]
    heads = w_key.shape[1] // nope
    head_nope = jnp.dot(normed, w_key, preferred_element_type=jnp.float32).astype(jnp.bfloat16)
    head_nope = head_nope.reshape(count, heads, nope)
    values = jnp.dot(normed, w_value, preferred_element_type=jnp.float32).astype(jnp.bfloat16)
    shared = rotary_key[:, None, :]
    joined = rms_scale(jnp.concatenate([head_nope, shared], axis=-1), key_gain)
    turned = rotate(joined[..., nope:], positions)
    keys_out = jnp.concatenate([joined[..., :nope], turned], axis=-1).astype(jnp.bfloat16)
    return (keys_out.reshape(count, -1), values)


def attend(state, queries, keys_in, values_in, depth):
    maxima, totals, weighted = state
    heads = maxima.shape[1]
    query_view = queries.reshape(queries.shape[0], heads, depth)
    key_view = keys_in.reshape(keys_in.shape[0], heads, depth)
    value_view = values_in.reshape(values_in.shape[0], heads, -1)
    scores = jnp.einsum(
        "qhd,khd->qhk", query_view, key_view, preferred_element_type=jnp.float32
    ) * depth ** (-0.5)
    new_max = jnp.maximum(maxima, jnp.max(scores, axis=-1))
    shifted = jnp.exp(scores - new_max[..., None])
    factor = jnp.exp(maxima - new_max)
    totals = totals * factor + jnp.sum(shifted, axis=-1)
    weighted = weighted * factor[..., None] + jnp.einsum(
        "qhk,khd->qhd", shifted.astype(jnp.bfloat16), value_view, preferred_element_type=jnp.float32
    )
    return (new_max, totals, weighted)


def in_blocks(carry, pieces, step_fn):
    length = pieces[0].shape[0]
    size = math.gcd(length, 1024)
    number = length // size
    stacked = tuple((member.reshape((number, size) + member.shape[1:]) for member in pieces))

    def advance(inner, item):
        position, parts = item
        return (step_fn(inner, parts, position * size), None)

    carry, unused = lax.scan(advance, carry, (jnp.arange(number, dtype=jnp.int32), stacked))
    return carry


def collect(w_up, w_down):
    return (
        lax.all_gather(w_up, "sp", axis=0, tiled=True),
        lax.all_gather(w_down, "sp", axis=1, tiled=True),
    )


def finish(group):
    maxima, totals, weighted = group
    return (weighted / totals[..., None]).astype(jnp.bfloat16).reshape(weighted.shape[0], -1)


def body(
    stream,
    query_a,
    query_b,
    latent,
    rotary_key,
    latent_gain,
    key_gain_a,
    key_gain_b,
    w_key_a,
    w_value_a,
    w_key_b,
    w_value_b,
    w_out_a,
    w_out_b,
    norm_gain,
    w_up,
    w_down,
):
    local = query_a.shape[0]
    depth_a = NOPE_A + ROPE
    depth_b = NOPE_B + ROPE
    heads_a = w_key_a.shape[1] // NOPE_A
    heads_b = w_key_b.shape[1] // NOPE_B

    def empty(heads, width):
        return (
            jnp.full((local, heads), -jnp.inf, jnp.float32),
            jnp.zeros((local, heads), jnp.float32),
            jnp.zeros((local, heads, width), jnp.float32),
        )

    start_state = (empty(heads_a, V_A), empty(heads_b, V_B))

    def attend_both(state, keys_a, values_a, keys_b, values_b):
        return (
            attend(state[0], query_a, keys_a, values_a, depth_a),
            attend(state[1], query_b, keys_b, values_b, depth_b),
        )

    def from_latent(state, pieces, start):
        latent_piece, rotary_piece = pieces
        positions = (start + jnp.arange(latent_piece.shape[0], dtype=jnp.int32)).astype(jnp.float32)
        normed_piece = rms_scale(latent_piece, latent_gain).astype(jnp.bfloat16)
        keys_a, values_a = make_keys(
            normed_piece, rotary_piece, w_key_a, w_value_a, key_gain_a, NOPE_A, positions
        )
        keys_b, values_b = make_keys(
            normed_piece, rotary_piece, w_key_b, w_value_b, key_gain_b, NOPE_B, positions
        )
        return attend_both(state, keys_a, values_a, keys_b, values_b)

    state = in_blocks(
        start_state,
        (
            lax.all_gather(latent, "sp", axis=0, tiled=True),
            lax.all_gather(rotary_key, "sp", axis=0, tiled=True),
        ),
        from_latent,
    )
    attended_a = finish(state[0])
    attended_b = finish(state[1])
    rows_a, rows_b = (
        lax.all_to_all(attended_a, "tp", split_axis=0, concat_axis=1, tiled=True),
        lax.all_to_all(attended_b, "tp", split_axis=0, concat_axis=1, tiled=True),
    )
    whole_a, whole_b = (
        lax.all_gather(w_out_a, "tp", axis=0, tiled=True),
        lax.all_gather(w_out_b, "tp", axis=0, tiled=True),
    )
    mixed = jnp.dot(rows_a, whole_a, preferred_element_type=jnp.float32) + jnp.dot(
        rows_b, whole_b, preferred_element_type=jnp.float32
    )
    residual = (stream.astype(jnp.float32) + mixed).astype(jnp.bfloat16)
    normed = rms_scale(residual, norm_gain).astype(jnp.bfloat16)
    up_full, down_full = collect(w_up, w_down)
    hidden = jnp.dot(
        lax.all_gather(normed, "tp", axis=0, tiled=True),
        up_full,
        preferred_element_type=jnp.float32,
    )
    activated = jnp.square(jax.nn.relu(hidden)).astype(jnp.bfloat16)
    summed = lax.psum_scatter(
        jnp.dot(activated, down_full, preferred_element_type=jnp.float32).astype(jnp.bfloat16),
        "tp",
        scatter_dimension=0,
        tiled=True,
    ).astype(jnp.float32)
    return (residual.astype(jnp.float32) + summed).astype(jnp.bfloat16)


def solution(mesh):
    in_specs = (
        P(("sp", "tp"), None),
        P("sp", "tp"),
        P("sp", "tp"),
        P("sp", None),
        P("sp", None),
        P(),
        P(),
        P(),
        P(None, "tp"),
        P(None, "tp"),
        P(None, "tp"),
        P(None, "tp"),
        P("tp", None),
        P("tp", None),
        P(),
        P("sp", "tp"),
        P("tp", "sp"),
    )
    out_specs = P(("sp", "tp"), None)
    return jax.shard_map(body, mesh=mesh, in_specs=in_specs, out_specs=out_specs, check_vma=False)
```

profile of v0, /device:TPU:0, one launch (start us, length us, event | category | flops | bytes accessed | tf_op | source)
XLA Modules:
  0.0 303.6 jit_solution(17043240091984500603)
XLA Ops:
  6.5 0.7 all-gather.7.cloned.1.call-update
  7.3 0.7 all-gather.9.cloned.1.call-update
  8.1 0.7 all-gather.11.cloned.1.call-update
  8.8 32.8 %all_gather.22 = bf16[2048,32]{0,1:T(8,128)(2,1)S(1)} all-gather(bf16[256,32]{0,1:T(8,128)(2,1)} %param.23), channel_id=1, replica_groups=mesh['sp'=8,'tp'=4] {'sp'}, dimensions={0}, use_global_device_ids=true | all-gather | bytes 147456 | tf_op jit(solution)/shard_map/all_gather | solution.py:151
  41.6 0.7 copy.36
  42.3 10.3 %all-gather.7.cloned.1.call-done = bf16[2048,256]{1,0:T(8,128)(2,1)} async-done(((bf16[256,256]{1,0:T(8,128)(2,1)}), bf16[2048,256]{1,0:T(8,128)(2,1)}) %all-gather.7.cloned.1.call-update) | async-done | bytes 1048592 | tf_op jit(solution)/shard_map/all_gather | solution.py:150
  52.6 0.5 iota.14
  53.1 23.9 %while.21 = (s32[]{:T(128)}, f32[256,1]{0,1:T(1,128)S(1)}, f32[256,1]{0,1:T(1,128)S(1)}, f32[256,1,64]{0,2,1:T(8,128)S(1)}, f32[256,1]{0,1:T(1,128)S(1)}, /*inde...) while((s32[]{:T(128)}, f32[256,1]{0,1:T(1,128)S(1)}, ...), condition=%wide.region_8.9_spmd.clone, body=%wide.region_0.8_spmd.clone.sunk | while | flops 449879584 | bytes 19054628 | solution.py:79
  53.1 1.3 fusion.141
  54.5 1.5 fusion.142
  55.9 0.9 dynamic-slice_bitcast_fusion.2
  56.8 0.1 fusion.143
  56.9 0.8 fusion.144
  57.7 1.5 fusion.145
  59.2 0.1 fusion.146
  59.3 0.1 fusion.147
  59.4 1.3 dynamic_slice.37
  61.4 0.3 fusion.148
  61.8 0.4 fusion.154
  62.2 0.2 fusion.156
  62.4 0.4 fusion.150
  62.8 0.2 fusion.152
  63.1 0.6 fusion.159
  63.7 1.3 fusion.158
  65.1 1.3 fusion.141
  66.4 1.5 fusion.142
  67.9 0.9 dynamic-slice_bitcast_fusion.2
  68.8 0.1 fusion.143
  68.9 0.8 fusion.144
  69.7 1.5 fusion.145
  71.2 0.1 fusion.146
  71.3 0.1 fusion.147
  71.4 1.3 dynamic_slice.37
  73.4 0.3 fusion.148
  73.8 0.4 fusion.154
  74.2 0.2 fusion.156
  74.4 0.4 fusion.150
  74.8 0.2 fusion.152
  75.1 0.6 fusion.159
  75.7 1.3 fusion.158
  77.1 0.1 copy.25
  77.2 0.1 copy.23
  77.3 0.7 reshape.462
  78.0 3.3 %all-to-all-start = ((bf16[4,2,2048]{2,1,0:T(2,128)(2,1)}), bf16[4,2,2048]{2,1,0:T(2,128)(2,1)S(1)}, u32[]{:S(2)}, u32[]{:S(2)}) async-start(bf16[4,2,2048]{2,1,0:T(2,128)(2,1)} %reshape.462), calls=%async_computation | async-start | bytes 65536 | tf_op jit(solution)/shard_map/all_to_all | solution.py:158
  81.3 0.7 divide_convert_fusion
  82.0 3.5 %all-to-all-done = bf16[4,2,2048]{2,1,0:T(2,128)(2,1)S(1)} async-done(((bf16[4,2,2048]{2,1,0:T(2,128)(2,1)}), bf16[4,2,2048]{2,1,0:T(2,128)(2,1)S(1)}, u32[]{:S(2)}, u32[]{:S(2)}) %all-to-all-start) | async-done | bytes 32800 | tf_op jit(solution)/shard_map/all_to_all | solution.py:158
  85.6 3.3 %all-to-all-start.1 = ((bf16[4,64,128]{2,1,0:T(8,128)(2,1)}), bf16[4,64,128]{2,1,0:T(8,128)(2,1)S(1)}, u32[]{:S(2)}, u32[]{:S(2)}) async-start(bf16[4,64,128]{2,1,0:T(8,128)(2,1)} %bitcast.5), calls=%async_computation.1 | async-start | bytes 131072 | tf_op jit(solution)/shard_map/all_to_all | solution.py:159
  88.9 0.0 all-gather.13.cloned.1.call-start
  88.9 0.1 reshape.463
  89.0 0.1 copy.24
  89.1 0.1 all_to_all.31
  89.2 1.5 fusion.84
  90.8 2.6 all-to-all-done.1
  93.4 1.4 all-gather.11.cloned.1.call-done
  94.8 2.2 multiply_reduce_fusion
  97.0 0.8 multiply_convert_fusion
  97.9 0.5 all-gather.15.cloned.1.call-update
  98.5 0.5 all-gather.17.cloned.1.call-update
  99.1 15.8 %all-gather.13.cloned.1.call-done = bf16[256,2048]{1,0:T(8,128)(2,1)} async-done(((bf16[64,2048]{1,0:T(8,128)(2,1)}), bf16[256,2048]{1,0:T(8,128)(2,1)}) %all-gather.13.cloned.1.call-update) | async-done | bytes 1048592 | tf_op jit(solution)/shard_map/all_gather | solution.py:172
  114.8 74.8 %all-gather.15.cloned.1.call-done = bf16[2048,1024]{1,0:T(8,128)(2,1)} async-done(((bf16[256,1024]{1,0:T(8,128)(2,1)}), bf16[2048,1024]{1,0:T(8,128)(2,1)}) %all-gather.15.cloned.1.call-update) | async-done | bytes 4194320 | tf_op jit(solution)/shard_map/all_gather | solution.py:85
  189.6 75.1 %all-gather.17.cloned.1.call-done = bf16[1024,2048]{1,0:T(8,128)(2,1)} async-done(((bf16[1024,256]{1,0:T(8,128)(2,1)}), bf16[1024,2048]{1,0:T(8,128)(2,1)}) %all-gather.17.cloned.1.call-update) | async-done | bytes 4194320 | tf_op jit(solution)/shard_map/all_gather | solution.py:86
  264.7 7.2 %convolution_convert_fusion.4 = bf16[256,2048]{1,0:T(8,128)(2,1)} fusion(bf16[1024,2048]{1,0:T(8,128)(2,1)} %all-gather.17.cloned.1.call-done, bf16[256,2048]{1,0:T(8,128)(2,1)} %all-gather.13.cloned.1.call-done, bf16[2048,1024]{1,0:T(8,128)(2,1)} %all-gather.15.cloned.1.call-done), kind=kOutput, calls=%fused_computation.99 | convolution fusion | flops 2148794368 | bytes 10485760 | tf_op jit(solution)/shard_map/dot_general | solution.py:178
  271.9 23.1 %reduce-scatter.2.cloned.1.call-done = bf16[64,2048]{1,0:T(8,128)(2,1)} async-done(((bf16[256,2048]{1,0:T(8,128)(2,1)}), bf16[64,2048]{1,0:T(8,128)(2,1)}) %reduce-scatter.2.cloned.1.call-update) | async-done | bytes 262160 | tf_op jit(solution)/shard_map/reduce_scatter | solution.py:177
  295.1 1.7 add_convert_fusion.1
  (67 shorter events, 0.6 us)
Async XLA Ops:
  6.5 46.1 %all-gather.7.cloned.1.call-start = ((), (), s32[]{:S(2)}) async-start(), calls=%async_computation.3 | async-start | bytes 1179648 | tf_op jit(solution)/shard_map/all_gather | solution.py:150
  7.3 82.0 %all-gather.9.cloned.1.call-start = ((), (), s32[]{:S(2)}) async-start(), calls=%async_computation.4 | async-start | bytes 1310720 | tf_op jit(solution)/shard_map/all_gather | solution.py:162
  8.0 86.8 %all-gather.11.cloned.1.call-start = ((), (), s32[]{:S(2)}) async-start(), calls=%async_computation.5 | async-start | bytes 2621440 | tf_op jit(solution)/shard_map/all_gather | solution.py:163
  53.1 6.2 %copy-start.4 = (f32[96]{0:T(128)S(1)}, f32[96]{0:T(128)}, u32[]{:S(2)}) copy-start(f32[96]{0:T(128)} %get-tuple-element.457) | copy-start | bytes 1156 | tf_op jit(solution)/shard_map/while
  53.1 8.7 %copy-start.6 = (bf16[256,160]{0,1:T(8,128)(2,1)S(1)}, bf16[256,160]{0,1:T(8,128)(2,1)}, u32[]{:S(2)}) copy-start(bf16[256,160]{0,1:T(8,128)(2,1)} %get-tuple-element.463) | copy-start | bytes 245764 | tf_op jit(solution)/shard_map/while
  54.4 8.0 %copy-start.2 = (bf16[256,96]{0,1:T(8,128)(2,1)S(1)}, bf16[256,96]{0,1:T(8,128)(2,1)}, u32[]{:S(2)}) copy-start(bf16[256,96]{0,1:T(8,128)(2,1)} %get-tuple-element.459) | copy-start | bytes 147460 | tf_op jit(solution)/shard_map/while
  57.7 5.4 %copy-start = (bf16[2,1024,256]{2,1,0:T(8,128)(2,1)S(1)}, bf16[2,1024,256]{2,1,0:T(8,128)(2,1)}, u32[]{:S(2)}) copy-start(bf16[2,1024,256]{2,1,0:T(8,128)(2,1)} %get-tuple-element.453) | copy-start | bytes 3145732 | tf_op jit(solution)/shard_map/while
  57.7 5.4 %copy-start.1 = (bf16[256,128]{1,0:T(8,128)(2,1)S(1)}, bf16[256,128]{1,0:T(8,128)(2,1)}, u32[]{:S(2)}) copy-start(bf16[256,128]{1,0:T(8,128)(2,1)} %get-tuple-element.464) | copy-start | bytes 196612 | tf_op jit(solution)/shard_map/while
  57.7 5.4 %copy-start.3 = (f32[256]{0:T(256)S(1)}, f32[256]{0:T(256)}, u32[]{:S(2)}) copy-start(f32[256]{0:T(256)} %get-tuple-element.454) | copy-start | bytes 3076 | tf_op jit(solution)/shard_map/while
  65.1 6.2 %copy-start.4 = (f32[96]{0:T(128)S(1)}, f32[96]{0:T(128)}, u32[]{:S(2)}) copy-start(f32[96]{0:T(128)} %get-tuple-element.457) | copy-start | bytes 1156 | tf_op jit(solution)/shard_map/while
  65.1 8.7 %copy-start.6 = (bf16[256,160]{0,1:T(8,128)(2,1)S(1)}, bf16[256,160]{0,1:T(8,128)(2,1)}, u32[]{:S(2)}) copy-start(bf16[256,160]{0,1:T(8,128)(2,1)} %get-tuple-element.463) | copy-start | bytes 245764 | tf_op jit(solution)/shard_map/while
  66.4 8.0 %copy-start.2 = (bf16[256,96]{0,1:T(8,128)(2,1)S(1)}, bf16[256,96]{0,1:T(8,128)(2,1)}, u32[]{:S(2)}) copy-start(bf16[256,96]{0,1:T(8,128)(2,1)} %get-tuple-element.459) | copy-start | bytes 147460 | tf_op jit(solution)/shard_map/while
  69.7 5.4 %copy-start = (bf16[2,1024,256]{2,1,0:T(8,128)(2,1)S(1)}, bf16[2,1024,256]{2,1,0:T(8,128)(2,1)}, u32[]{:S(2)}) copy-start(bf16[2,1024,256]{2,1,0:T(8,128)(2,1)} %get-tuple-element.453) | copy-start | bytes 3145732 | tf_op jit(solution)/shard_map/while
  69.7 5.4 %copy-start.1 = (bf16[256,128]{1,0:T(8,128)(2,1)S(1)}, bf16[256,128]{1,0:T(8,128)(2,1)}, u32[]{:S(2)}) copy-start(bf16[256,128]{1,0:T(8,128)(2,1)} %get-tuple-element.464) | copy-start | bytes 196612 | tf_op jit(solution)/shard_map/while
  69.7 5.4 %copy-start.3 = (f32[256]{0:T(256)S(1)}, f32[256]{0:T(256)}, u32[]{:S(2)}) copy-start(f32[256]{0:T(256)} %get-tuple-element.454) | copy-start | bytes 3076 | tf_op jit(solution)/shard_map/while
  77.1 20.0 %copy-start.5 = (f32[2048]{0:T(1024)S(1)}, f32[2048]{0:T(1024)}, u32[]{:S(2)}) copy-start(f32[2048]{0:T(1024)} %param.33) | copy-start | bytes 24580
  78.0 7.6 %all-to-all-start = ((bf16[4,2,2048]{2,1,0:T(2,128)(2,1)}), bf16[4,2,2048]{2,1,0:T(2,128)(2,1)S(1)}, u32[]{:S(2)}, u32[]{:S(2)}) async-start(bf16[4,2,2048]{2,1,0:T(2,128)(2,1)} %reshape.462), calls=%async_computation | async-start | bytes 65536 | tf_op jit(solution)/shard_map/all_to_all | solution.py:158
  85.6 7.8 %all-to-all-start.1 = ((bf16[4,64,128]{2,1,0:T(8,128)(2,1)}), bf16[4,64,128]{2,1,0:T(8,128)(2,1)S(1)}, u32[]{:S(2)}, u32[]{:S(2)}) async-start(bf16[4,64,128]{2,1,0:T(8,128)(2,1)} %bitcast.5), calls=%async_computation.1 | async-start | bytes 131072 | tf_op jit(solution)/shard_map/all_to_all | solution.py:159
  88.9 26.0 %all-gather.13.cloned.1.call-start = ((), (), s32[]{:S(2)}) async-start(), calls=%async_computation.6 | async-start | bytes 1310720 | tf_op jit(solution)/shard_map/all_gather | solution.py:172
  97.9 91.8 %all-gather.15.cloned.1.call-start = ((), (), s32[]{:S(2)}) async-start(), calls=%async_computation.7 | async-start | bytes 4718592 | tf_op jit(solution)/shard_map/all_gather | solution.py:85
  98.5 166.3 %all-gather.17.cloned.1.call-start = ((), (), s32[]{:S(2)}) async-start(), calls=%async_computation.8 | async-start | bytes 4718592 | tf_op jit(solution)/shard_map/all_gather | solution.py:86
  99.0 196.0 %reduce-scatter.2.cloned.1.call-start = ((), (), s32[]{:S(2)}) async-start(), calls=%async_computation.9 | async-start | bytes 1310720 | tf_op jit(solution)/shard_map/reduce_scatter | solution.py:177
Sparse Core Ops, SparseCore 0:
  9.5 43.1 all-gather.6
  54.2 15.3 all-gather.8
  71.1 23.5 all-gather.10
  98.0 16.8 all-gather.12
  116.8 72.7 all-gather.14
  191.5 73.1 all-gather.16
  272.1 22.9 reduce-scatter.1
where the time goes:
time: 304 us
  waiting for transfers between devices  210 us (69%)
  blocking collectives  32.8 us (11%)
  matrix products  22.2 us (7%)
  between operations  13.6 us (4%)
  other arithmetic  9.61 us (3%)
  local copies, waits for them, and re-layouts  6.83 us (2%)
  starting transfers between devices  6.79 us (2%)
    all_gather x1, waiting for transfers between devices, collect(): lax.all_gather(w_down, 'sp', axis=1, tiled=True)  75.1 us
    all_gather x1, waiting for transfers between devices, collect(): lax.all_gather(w_up, 'sp', axis=0, tiled=True)  74.8 us
    all_gather x1, blocking collectives, body(): lax.all_gather(rotary_key, 'sp', axis=0, tiled=True)  32.8 us
    reduce_scatter x1, waiting for transfers between devices, body(): lax.psum_scatter(jnp.dot(activated, down_full, preferred_element_type=jnp...  23.1 us
    all_gather x1, waiting for transfers between devices, body(): lax.all_gather(normed, 'tp', axis=0, tiled=True)  15.8 us
    all_gather x1, waiting for transfers between devices, body(): lax.all_gather(latent, 'sp', axis=0, tiled=True)  10.3 us
    dot_general x1, matrix products, body(): jnp.dot(activated, down_full, preferred_element_type=jnp.float32)  7.18 us
  transfers between devices with their start and end apart: 9, of which 8 were waited for; matrix products, arithmetic and copies ran while one was open for 9% of the time, Pallas kernels for 0%

commit v1 on v0

v1 whole, which is shorter than its diff:
```python
import functools

import jax
import jax.numpy as jnp
from jax import lax
from jax.experimental import pallas as pl
from jax.experimental.pallas import tpu as pltpu
from jax.sharding import PartitionSpec as P

NOPE_A = 64
V_A = 64
NOPE_B = 128
V_B = 128
ROPE = 32

EPSILON = 1e-06
THETA = 10000.0
F32 = jnp.float32
BF16 = jnp.bfloat16


def kernel(
    n, m,
    stream, q_a, q_b, packed, table, lat_gain, gain_a, gain_b,
    wk_a, wv_a, wk_b, wv_b, wo_a, wo_b, norm_gain, w_up, w_down,
    out,
    lat, key_a, key_b, val_a, val_b, att, rows, goa, gob,
    gup, gdown, x, hid, act, res, even, odd, sib, mid, part, land,
    lat_s, lat_r, latf_s, latf_r, oa_s, oa_r, ob_s, ob_r,
    up_s, up_r, dn_s, dn_r, at_s, at_r, x_s, x_r, rs_s, rs_r,
):
    s = lax.axis_index("sp")
    t = lax.axis_index("tp")
    core = t & 1
    length = q_a.shape[0]
    own = stream.shape[0]
    prow = packed.shape[0]
    half_rows = prow // 2
    depth_a = NOPE_A + ROPE
    depth_b = NOPE_B + ROPE
    heads_a = wk_a.shape[1] // NOPE_A
    heads_b = wk_b.shape[1] // NOPE_B
    hidden = gup.shape[2]
    wrows = w_up.shape[0]
    wcols = w_down.shape[1]
    width_a = heads_a * V_A
    width_b = heads_b * V_B
    start_b = att.shape[2] - width_b
    pending = []

    def copy(src, dst, ssem, rsem, sp, tp):
        return pltpu.make_async_remote_copy(
            src_ref=src, dst_ref=dst, send_sem=ssem, recv_sem=rsem,
            device_id={"sp": sp, "tp": tp}, device_id_type=pl.DeviceIdType.MESH,
        )

    def send(*args):
        c = copy(*args)
        c.start()
        pending.append(c)

    barrier = pltpu.get_barrier_semaphore()
    for k in range(1, n):
        pl.semaphore_signal(barrier, inc=1, device_id={"sp": s ^ k, "tp": t},
                            device_id_type=pl.DeviceIdType.MESH)
    for k in range(1, m):
        pl.semaphore_signal(barrier, inc=1, device_id={"sp": s, "tp": t ^ k},
                            device_id_type=pl.DeviceIdType.MESH)
    pl.semaphore_wait(barrier, n + m - 2)

    mine = pl.ds(pl.multiple_of(core * half_rows, 16), half_rows)
    other = pl.ds(pl.multiple_of((1 - core) * half_rows, 16), half_rows)
    for k in range(1, n):
        send(packed.at[mine], lat.at[k, mine], lat_s.at[k], lat_r.at[k], s ^ k, t)
    for k in (2, 1):
        send(wo_a, goa.at[k - 1], oa_s.at[k - 1], oa_r.at[k - 1], s, t ^ k)
        send(wo_b, gob.at[k - 1], ob_s.at[k - 1], ob_r.at[k - 1], s, t ^ k)

    def halves(target):
        return pl.ds(pl.multiple_of(((target // 2) % 2) * hidden, 128), hidden)

    for k in [1] + list(range(2, n, 2)):
        send(w_up.at[:, halves(s ^ k)], gup.at[k], up_s.at[k], up_r.at[k], s ^ k, t)
    for k in [1] + list(range(2, n, 2)):
        send(w_down.at[halves(s ^ k)], gdown.at[k], dn_s.at[k], dn_r.at[k], s ^ k, t)

    def make_block(k, source):
        start = pl.multiple_of(k * length, length)
        at = pl.ds(start, length)
        wide = source[0:length, :].astype(F32)
        normed = (wide * lax.rsqrt(jnp.mean(wide * wide, axis=-1, keepdims=True) + EPSILON)
                  * lat_gain[...]).astype(BF16)
        tail = source[length:prow, :].astype(F32)
        lanes = tail.shape[1] // ROPE
        rotary = jnp.concatenate([tail[:, i * ROPE:(i + 1) * ROPE] for i in range(lanes)], axis=0)
        squares = jnp.sum(rotary * rotary, axis=-1, keepdims=True)
        turn = table[s ^ k]
        half = ROPE // 2

        def keys(wk, gain, nope, heads, dest):
            flat = jnp.dot(normed, wk[...], preferred_element_type=F32).astype(BF16).astype(F32)
            for h in range(heads):
                piece = flat[:, h * nope:(h + 1) * nope]
                mean = (jnp.sum(piece * piece, axis=-1, keepdims=True) + squares) / (nope + ROPE)
                scale = lax.rsqrt(mean + EPSILON)
                dest[h, at, 0:nope] = (piece * scale * gain[:, 0:nope]).astype(BF16)
                last = rotary * scale * gain[:, nope:nope + ROPE]
                swapped = jnp.concatenate([last[:, half:], last[:, :half]], axis=-1)
                dest[h, at, nope:nope + ROPE] = (
                    last * turn[:, 0:ROPE] + swapped * turn[:, ROPE:2 * ROPE]).astype(BF16)

        keys(wk_a, gain_a, NOPE_A, heads_a, key_a)
        keys(wk_b, gain_b, NOPE_B, heads_b, key_b)
        val_a[at, :] = jnp.dot(normed, wv_a[...], preferred_element_type=F32).astype(BF16)
        val_b[at, :] = jnp.dot(normed, wv_b[...], preferred_element_type=F32).astype(BF16)

    make_block(0, packed)
    for k in range(1, n):
        copy(packed.at[mine], lat.at[k, mine], lat_s.at[k], lat_r.at[k], s ^ k, t).wait_recv()
        send(lat.at[k, mine], lat.at[k, mine], latf_s.at[k], latf_r.at[k], s, t ^ 1)
    copy(wo_a, goa.at[1], oa_s.at[1], oa_r.at[1], s, t ^ 2).wait_recv()
    send(goa.at[1], goa.at[2], oa_s.at[2], oa_r.at[2], s, t ^ 1)
    copy(wo_b, gob.at[1], ob_s.at[1], ob_r.at[1], s, t ^ 2).wait_recv()
    send(gob.at[1], gob.at[2], ob_s.at[2], ob_r.at[2], s, t ^ 1)

    def one(k, carry):
        copy(lat.at[k, other], lat.at[k, other], latf_s.at[k], latf_r.at[k], s, t ^ 1).wait_recv()
        make_block(k, lat.at[k])
        return carry

    lax.fori_loop(1, n, one, 0)

    total = n * length
    block = min(total, 2048)
    number = total // block

    def attend(q, key, value, h, depth, width):
        query = q[:, h * depth:(h + 1) * depth]

        def step(i, state):
            peak, sums, acc = state
            at = pl.ds(pl.multiple_of(i * block, block), block)
            score = lax.dot_general(query, key[h, at, :], (((1,), (1,)), ((), ())),
                                    preferred_element_type=F32) * depth ** (-0.5)
            new = jnp.maximum(peak, jnp.max(score, axis=-1, keepdims=True))
            shifted = jnp.exp(score - new)
            factor = jnp.exp(peak - new)
            sums = sums * factor + jnp.sum(shifted, axis=-1, keepdims=True)
            acc = acc * factor + jnp.dot(
                shifted.astype(BF16), value[at, h * width:(h + 1) * width],
                preferred_element_type=F32)
            return new, sums, acc

        state = (jnp.full((length, 1), -jnp.inf, F32), jnp.zeros((length, 1), F32),
                 jnp.zeros((length, width), F32))
        if number == 1:
            state = step(0, state)
        else:
            state = lax.fori_loop(0, number, step, state)
        return (state[2] / state[1]).astype(BF16)

    for h in range(heads_a):
        res_a = attend(q_a, key_a, val_a, h, depth_a, V_A)
        for j in range(m):
            att[j, :, h * V_A:(h + 1) * V_A] = res_a[j * own:(j + 1) * own]
    for h in range(heads_b):
        res_b = attend(q_b, key_b, val_b, h, depth_b, V_B)
        for j in range(m):
            att[j, :, start_b + h * V_B:start_b + (h + 1) * V_B] = res_b[j * own:(j + 1) * own]
    for k in range(1, m):
        send(att.at[t ^ k], rows.at[k], at_s.at[k], at_r.at[k], s, t ^ k)

    for k in range(2, n, 2):
        copy(gup.at[k], gup.at[k], up_s.at[k], up_r.at[k], s ^ k, t).wait_recv()
        send(gup.at[k], gup.at[k + 1], up_s.at[k + 1], up_r.at[k + 1], s ^ 1, t)

    mixed = (jnp.dot(att[t, :, 0:width_a], wo_a[...], preferred_element_type=F32)
             + jnp.dot(att[t, :, start_b:], wo_b[...], preferred_element_type=F32))
    for k in range(1, m):
        copy(wo_a, goa.at[k - 1], oa_s.at[k - 1], oa_r.at[k - 1], s, t ^ 1) \
            .wait_recv() if k != 2 else None
        copy(wo_b, gob.at[k - 1], ob_s.at[k - 1], ob_r.at[k - 1], s, t ^ 1) \
            .wait_recv() if k != 2 else None
        copy(att.at[t ^ k], rows.at[k], at_s.at[k], at_r.at[k], s, t ^ k).wait_recv()
        mixed += jnp.dot(rows[k, :, 0:width_a], goa[k - 1], preferred_element_type=F32)
        mixed += jnp.dot(rows[k, :, start_b:], gob[k - 1], preferred_element_type=F32)
    residual = (stream[...].astype(F32) + mixed).astype(BF16)
    res[...] = residual
    wide = residual.astype(F32)
    x[0:own, :] = (wide * lax.rsqrt(jnp.mean(wide * wide, axis=-1, keepdims=True) + EPSILON)
                   * norm_gain[...]).astype(BF16)

    def peer(code):
        return (s ^ 2 if code & 4 else s), t ^ (code & 3)

    def slot(k):
        return x.at[pl.ds(k * own, own)]

    def xcopy(src, dst, code):
        return copy(slot(src), slot(dst), x_s.at[dst], x_r.at[dst], *peer(code))

    def xsend(src, dst, code):
        c = xcopy(src, dst, code)
        c.start()
        pending.append(c)

    for code in (2, 4, 1):
        xsend(0, code, code)
    xcopy(0, 2, 2).wait_recv()
    xcopy(0, 4, 4).wait_recv()
    diag = copy(
        x.at[pl.ds(pl.multiple_of((2 + 2 * core) * own, own), own)], slot(6),
        x_s.at[6], x_r.at[6], s ^ (2 - 2 * core), t ^ (2 * core))
    diag.start()
    pending.append(diag)
    xsend(2, 3, 1)
    xsend(4, 5, 1)
    diag.wait_recv()
    xsend(6, 7, 1)
    for k in range(2, n, 2):
        copy(gdown.at[k], gdown.at[k], dn_s.at[k], dn_r.at[k], s ^ k, t).wait_recv()
        send(gdown.at[k], gdown.at[k + 1], dn_s.at[k + 1], dn_r.at[k + 1], s ^ 1, t)
    for k in (1, 3, 5, 7):
        xcopy(k - 1, k, 1).wait_recv()

    def columns(k, size):
        return pl.ds(pl.multiple_of((s ^ k) * size, 128), size)

    held = halves(s)
    hid[...] = jnp.dot(x[:, columns(0, wrows)], w_up[:, held], preferred_element_type=F32)
    for k in [1] + list(range(3, n, 2)):
        copy(gup.at[k], gup.at[k], up_s.at[k], up_r.at[k], s ^ 1, t).wait_recv()

    def up(k, carry):
        hid[...] += jnp.dot(x[:, columns(k, wrows)], gup[k], preferred_element_type=F32)
        return carry

    lax.fori_loop(1, n, up, 0)
    act[...] = jnp.square(jnp.maximum(hid[...], 0.0)).astype(BF16)
    for k in [1] + list(range(3, n, 2)):
        copy(gdown.at[k], gdown.at[k], dn_s.at[k], dn_r.at[k], s ^ 1, t).wait_recv()

    def split(k, piece):
        at = columns(k, wcols)
        for i in range(4):
            even[i, :, at] = piece[2 * i * own:(2 * i + 1) * own]
            odd[i, :, at] = piece[(2 * i + 1) * own:(2 * i + 2) * own].astype(BF16)

    split(0, jnp.dot(act[...], w_down[held, :], preferred_element_type=F32))

    def down(k, carry):
        split(k, jnp.dot(act[...], gdown[k], preferred_element_type=F32))
        return carry

    lax.fori_loop(1, n, down, 0)

    first = copy(odd, sib, rs_s.at[0], rs_r.at[0], s, t ^ 1)
    first.start()
    pending.append(first)
    first.wait_recv()
    mid[...] = (even[3] + sib[3].astype(F32)).astype(BF16)
    second = copy(mid, land.at[0], rs_s.at[1], rs_r.at[1], s ^ (2 - 2 * core), t ^ (2 * core))
    second.start()
    pending.append(second)
    for i in range(3):
        even[i] += sib[i].astype(F32)
    second.wait_recv()
    even[1 + core] += land[0].astype(F32)
    for i in (1, 2):
        part[i - 1] = even[i].astype(BF16)
    third = copy(part.at[0], land.at[1], rs_s.at[2], rs_r.at[2], s, t ^ 2)
    third.start()
    fourth = copy(part.at[1], land.at[2], rs_s.at[3], rs_r.at[3], s ^ 2, t)
    fourth.start()
    pending.append(third)
    pending.append(fourth)
    third.wait_recv()
    fourth.wait_recv()
    summed = even[0] + land[1].astype(F32) + land[2].astype(F32)
    out[...] = (res[...].astype(F32) + summed).astype(BF16)
    for c in pending:
        c.wait_send()


def body(n, m, stream, query_a, query_b, latent, rotary_key, latent_gain, key_gain_a, key_gain_b,
         w_key_a, w_value_a, w_key_b, w_value_b, w_out_a, w_out_b, norm_gain, w_up, w_down):
    length, rank = latent.shape
    own, features = stream.shape
    lanes = rank // ROPE
    tail = rotary_key.reshape(lanes, length // lanes, ROPE).transpose(1, 0, 2)
    packed = jnp.concatenate([latent, tail.reshape(length // lanes, rank)], axis=0)
    half = ROPE // 2
    freqs = THETA ** (-jnp.arange(half, dtype=F32) / half)
    angle = jnp.arange(n * length, dtype=jnp.int32).astype(F32)[:, None] * freqs
    cosine, sine = jnp.cos(angle), jnp.sin(angle)
    table = jnp.concatenate([cosine, cosine, -sine, sine], axis=-1).reshape(n, length, 2 * ROPE)
    total = n * length
    heads_a = w_key_a.shape[1] // NOPE_A
    heads_b = w_key_b.shape[1] // NOPE_B
    width_a = -(-heads_a * V_A // 128) * 128
    width_b = heads_b * V_B
    hidden = w_up.shape[1] // 2
    V = pltpu.VMEM
    dma = lambda k: pltpu.SemaphoreType.DMA((k,))
    tokens = 2 * m * own
    scratch = [
        V((n,) + packed.shape, BF16),
        V((heads_a, total, NOPE_A + ROPE), BF16),
        V((heads_b, total, NOPE_B + ROPE), BF16),
        V((total, heads_a * V_A), BF16),
        V((total, heads_b * V_B), BF16),
        V((m, own, width_a + width_b), BF16),
        V((m, own, width_a + width_b), BF16),
        V((m - 1,) + w_out_a.shape, BF16),
        V((m - 1,) + w_out_b.shape, BF16),
        V((n, w_up.shape[0], hidden), BF16),
        V((n, hidden, w_down.shape[1]), BF16),
        V((tokens, features), BF16),
        V((tokens, hidden), F32),
        V((tokens, hidden), BF16),
        V((own, features), BF16),
        V((m, own, features), F32),
        V((m, own, features), BF16),
        V((m, own, features), BF16),
        V((own, features), BF16),
        V((2, own, features), BF16),
        V((3, own, features), BF16),
    ]
    sizes = [n, n, n, n, 3, 3, 3, 3, n, n, n, n, m, m, 8, 8, 4, 4]
    scratch += [dma(k) for k in sizes]
    return pl.pallas_call(
        functools.partial(kernel, n, m),
        out_shape=jax.ShapeDtypeStruct((own, features), BF16),
        in_specs=[pl.BlockSpec(memory_space=V)] * 17,
        out_specs=pl.BlockSpec(memory_space=V),
        scratch_shapes=scratch,
        compiler_params=pltpu.CompilerParams(
            collective_id=0, has_side_effects=True, vmem_limit_bytes=67043328),
        name="layer",
    )(stream, query_a, query_b, packed, table, latent_gain[None], key_gain_a[None],
      key_gain_b[None], w_key_a, w_value_a, w_key_b, w_value_b, w_out_a, w_out_b,
      norm_gain[None], w_up, w_down)


def solution(mesh):
    n, m = mesh.shape["sp"], mesh.shape["tp"]
    in_specs = (
        P(("sp", "tp"), None),
        P("sp", "tp"),
        P("sp", "tp"),
        P("sp", None),
        P("sp", None),
        P(),
        P(),
        P(),
        P(None, "tp"),
        P(None, "tp"),
        P(None, "tp"),
        P(None, "tp"),
        P("tp", None),
        P("tp", None),
        P(),
        P("sp", "tp"),
        P("tp", "sp"),
    )
    out_specs = P(("sp", "tp"), None)
    return jax.shard_map(functools.partial(body, n, m), mesh=mesh, in_specs=in_specs,
                         out_specs=out_specs, check_vma=False)
```

time: 304 us -> 119 us (0.39)
  waiting for transfers between devices: 210 us -> 0 us
  Pallas kernels: 0 us -> 106 us
  blocking collectives: 32.8 us -> 0 us
  matrix products: 22.2 us -> 0 us
  between operations: 13.6 us -> 0.04 us
  starting transfers between devices: 6.79 us -> 0 us
  other arithmetic: 9.61 us -> 6.26 us
    all_gather x6 -> x0, waiting for transfers between devices: 177 us -> none  [the longest x1 75.1 us: collect(): lax.all_gather(w_down, 'sp', axis=1, tiled=True)]
    pallas_call x0 -> x1, Pallas kernels: none -> 106 us  [body(): pl.pallas_call(functools.partial(kernel, n, m), out_shape=jax.ShapeDtypeS...]
    all_gather x1 -> x0, blocking collectives: 32.8 us -> none  [body(): lax.all_gather(rotary_key, 'sp', axis=0, tiled=True)]
    reduce_scatter x1 -> x0, waiting for transfers between devices: 23.1 us -> none  [body(): lax.psum_scatter(jnp.dot(activated, down_full, preferred_element_type=jnp...]
    dot_general x15 -> x0, matrix products: 22.2 us -> none  [the longest x1 7.18 us: body(): jnp.dot(activated, down_full, preferred_element_type=jnp.float32)]
    all_to_all x2 -> x0, starting transfers between devices: 6.55 us -> none  [the longest x1 3.29 us: body(): lax.all_to_all(attended_b, 'tp', split_axis=0, concat_axis=1, tiled=True)]
    all_to_all x2 -> x0, waiting for transfers between devices: 6.14 us -> none  [the longest x1 3.54 us: body(): lax.all_to_all(attended_a, 'tp', split_axis=0, concat_axis=1, tiled=True)]
    unnamed x4 -> x17, local copies, waits for them, and re-layouts: 0.84 us -> 5.51 us
  transfers between devices with their start and end apart: 9 -> 0, of which waited for: 8 -> 0; matrix products, arithmetic and copies ran while one was open for 9% -> 0% of each run, Pallas kernels for 0% -> 0%
where the time goes in v1:
time: 119 us; the launch traced here: 118 us
  Pallas kernels  106 us (89%)
  other arithmetic  6.26 us (5%)
  local copies, waits for them, and re-layouts  5.84 us (5%)
    pallas_call x1, Pallas kernels, body(): pl.pallas_call(functools.partial(kernel, n, m), out_shape=jax.ShapeDtypeS...  106 us
    unnamed x17, local copies, waits for them, and re-layouts  5.51 us
    cos x1, other arithmetic, body(): cosine, sine = (jnp.cos(angle), jnp.sin(angle))  3.72 us

profile of v1, /device:TPU:0, one launch (start us, length us, event | category | flops | bytes accessed | tf_op | source)
XLA Modules:
  0.0 118.4 jit_solution(4470517591548724012)
XLA Ops:
  0.0 3.7 %multiply_cosine_fusion = (f32[8,256,16]{2,1,0:T(8,128)S(1)}, f32[8,256,16]{2,1,0:T(8,128)S(1)}, f32[8,256,16]{2,1,0:T(8,128)S(1)}) fusion(f32[16]{0:T(128)S(1)} %multiply_power_fusion, f32[8,256]{1,0:T(8,128)S(1)} %add_convert_fusion), kind=kLoop, calls=%fused_computation.1 | loop fusion | flops 65536 | bytes 401472 | tf_op jit(solution)/shard_map/cos | solution.py:295
  3.7 0.0 copy-start.5
  3.8 1.9 %pad_maximum_fusion.table = f32[8,256,64]{2,1,0:T(8,128)} fusion(f32[8,256,16]{2,1,0:T(8,128)S(1)} %get-tuple-element.7, f32[8,256,16]{2,1,0:T(8,128)S(1)} %get-tuple-element.6, f32[8,256,16]{2,1,0:T(8,128)S(1)} %get-tuple-element.5), kind=kLoop, calls=%fused_computation.2 | loop fusion | flops 393216 | bytes 917504 | tf_op jit(solution)/shard_map/concatenate | solution.py:296
  5.6 0.0 copy-done.5
  5.6 0.0 copy-start
  5.6 0.1 reshape.61
  5.7 0.1 copy.23
  5.9 0.1 reshape.62
  6.0 0.6 copy-done
  6.5 0.0 copy-start.1
  6.5 0.7 pad_maximum_fusion.1.packed
  7.2 0.2 copy-done.1
  7.4 0.0 copy-start.2
  7.4 0.8 copy.26.q_b
  8.2 0.0 copy-done.2
  8.2 0.0 copy-start.3
  8.2 0.7 copy.25.q_a
  9.0 0.0 copy-done.3
  9.0 0.0 copy-start.4
  9.0 0.7 copy.27.wk_a
  9.7 0.0 copy-done.4
  9.7 0.7 copy.28.wv_a
  10.5 106.2 %layer.1 = bf16[64,2048]{1,0:T(8,128)(2,1)} custom-call(bf16[64,2048]{1,0:T(8,128)(2,1)} %stream.1, bf16[256,96]{1,0:T(8,128)(2,1)} %copy.25.q_a, bf16[256,160]{1,0:T(8,128)(2,1)} %copy.26.q_b, bf16[288,256]{1,0:T(8,128)(2,1)} %pad_maximum_fusion.1.packed, f32[8,256,64]{2,1,0:T(8,128)} %pad_maximum_fusion.table, f32[1,256]{1,0:T(1,128)} %bitcast.9, ...), custom_call_target="tpu_custom_call" | custom-call | tf_op jit(solution)/shard_map/layer/pallas_call | solution.py:331
  116.7 1.7 %copy.30 = bf16[64,2048]{1,0:T(8,128)(2,1)} copy(bf16[64,2048]{1,0:T(8,128)(2,1)} %layer.1) | data formatting | bytes 524288
  (2 shorter events, 0.0 us)
Async XLA Ops:
  3.7 1.9 %copy-start.5 = (bf16[256,32]{0,1:T(8,128)(2,1)S(1)}, bf16[256,32]{0,1:T(8,128)(2,1)}, u32[]{:S(2)}) copy-start(bf16[256,32]{0,1:T(8,128)(2,1)} %param.21) | copy-start | bytes 49156
  5.6 0.9 copy-start
  6.5 0.9 copy-start.1
  7.4 0.8 copy-start.2
  8.2 0.8 copy-start.3
  9.0 0.8 copy-start.4

commit v2 on v1

--- a/solution.py
+++ b/solution.py
@@ -2,6 +2,7 @@
 
 import jax
 import jax.numpy as jnp
+import numpy as np
 from jax import lax
 from jax.experimental import pallas as pl
 from jax.experimental.pallas import tpu as pltpu
@@ -32,13 +33,13 @@
     s = lax.axis_index("sp")
     t = lax.axis_index("tp")
     core = t & 1
-    length = q_a.shape[0]
+    length = q_a.shape[1]
     own = stream.shape[0]
     prow = packed.shape[0]
     half_rows = prow // 2
     depth_a = NOPE_A + ROPE
     depth_b = NOPE_B + ROPE
-    heads_a = wk_a.shape[1] // NOPE_A
+    heads_a = wk_a.shape[0] // NOPE_A
     heads_b = wk_b.shape[1] // NOPE_B
     hidden = gup.shape[2]
     wrows = w_up.shape[0]
@@ -70,7 +71,7 @@
 
     mine = pl.ds(pl.multiple_of(core * half_rows, 16), half_rows)
     other = pl.ds(pl.multiple_of((1 - core) * half_rows, 16), half_rows)
-    for k in range(1, n):
+    for k in [1] + list(range(2, n, 2)):
         send(packed.at[mine], lat.at[k, mine], lat_s.at[k], lat_r.at[k], s ^ k, t)
     for k in (2, 1):
         send(wo_a, goa.at[k - 1], oa_s.at[k - 1], oa_r.at[k - 1], s, t ^ k)
@@ -94,11 +95,17 @@
         lanes = tail.shape[1] // ROPE
         rotary = jnp.concatenate([tail[:, i * ROPE:(i + 1) * ROPE] for i in range(lanes)], axis=0)
         squares = jnp.sum(rotary * rotary, axis=-1, keepdims=True)
+        half = ROPE // 2
         turn = table[s ^ k]
-        half = ROPE // 2
-
-        def keys(wk, gain, nope, heads, dest):
-            flat = jnp.dot(normed, wk[...], preferred_element_type=F32).astype(BF16).astype(F32)
+        cosine = jnp.concatenate([turn[:, :half], turn[:, :half]], axis=-1)
+        sine = jnp.concatenate([-turn[:, half:], turn[:, half:]], axis=-1)
+
+        def turned(w):
+            return lax.dot_general(normed, w[...], (((1,), (1,)), ((), ())),
+                                   preferred_element_type=F32)
+
+        def keys(flat, gain, nope, heads, dest):
+            flat = flat.astype(BF16).astype(F32)
             for h in range(heads):
                 piece = flat[:, h * nope:(h + 1) * nope]
                 mean = (jnp.sum(piece * piece, axis=-1, keepdims=True) + squares) / (nope + ROPE)
@@ -107,21 +114,34 @@
                 last = rotary * scale * gain[:, nope:nope + ROPE]
                 swapped = jnp.concatenate([last[:, half:], last[:, :half]], axis=-1)
                 dest[h, at, nope:nope + ROPE] = (
-                    last * turn[:, 0:ROPE] + swapped * turn[:, ROPE:2 * ROPE]).astype(BF16)
-
-        keys(wk_a, gain_a, NOPE_A, heads_a, key_a)
-        keys(wk_b, gain_b, NOPE_B, heads_b, key_b)
-        val_a[at, :] = jnp.dot(normed, wv_a[...], preferred_element_type=F32).astype(BF16)
+                    last * cosine + swapped * sine).astype(BF16)
+
+        keys(turned(wk_a), gain_a, NOPE_A, heads_a, key_a)
+        keys(jnp.dot(normed, wk_b[...], preferred_element_type=F32), gain_b, NOPE_B, heads_b, key_b)
+        val_a[at, :] = turned(wv_a).astype(BF16)
         val_b[at, :] = jnp.dot(normed, wv_b[...], preferred_element_type=F32).astype(BF16)
 
     make_block(0, packed)
-    for k in range(1, n):
+    def arrived(k):
         copy(packed.at[mine], lat.at[k, mine], lat_s.at[k], lat_r.at[k], s ^ k, t).wait_recv()
+
+    def to_sibling(k):
         send(lat.at[k, mine], lat.at[k, mine], latf_s.at[k], latf_r.at[k], s, t ^ 1)
-    copy(wo_a, goa.at[1], oa_s.at[1], oa_r.at[1], s, t ^ 2).wait_recv()
-    send(goa.at[1], goa.at[2], oa_s.at[2], oa_r.at[2], s, t ^ 1)
-    copy(wo_b, gob.at[1], ob_s.at[1], ob_r.at[1], s, t ^ 2).wait_recv()
-    send(gob.at[1], gob.at[2], ob_s.at[2], ob_r.at[2], s, t ^ 1)
+
+    arrived(1)
+    to_sibling(1)
+    for k in range(2, n, 2):
+        arrived(k)
+        send(lat.at[k, mine], lat.at[k + 1, mine], lat_s.at[k + 1], lat_r.at[k + 1], s ^ 1, t)
+        to_sibling(k)
+
+    def weights_on(ref, ssem, rsem, k):
+        copy(ref.at[k], ref.at[k], ssem.at[k], rsem.at[k], s ^ k, t).wait_recv()
+        send(ref.at[k], ref.at[k + 1], ssem.at[k + 1], rsem.at[k + 1], s ^ 1, t)
+
+    for k in range(3, n, 2):
+        arrived(k)
+        to_sibling(k)
 
     def one(k, carry):
         copy(lat.at[k, other], lat.at[k, other], latf_s.at[k], latf_r.at[k], s, t ^ 1).wait_recv()
@@ -129,13 +149,14 @@
         return carry
 
     lax.fori_loop(1, n, one, 0)
+    weights_on(gup, up_s, up_r, 2)
 
     total = n * length
     block = min(total, 2048)
     number = total // block
 
     def attend(q, key, value, h, depth, width):
-        query = q[:, h * depth:(h + 1) * depth]
+        query = q[h * depth:(h + 1) * depth, :].T
 
         def step(i, state):
             peak, sums, acc = state
@@ -163,16 +184,17 @@
         res_a = attend(q_a, key_a, val_a, h, depth_a, V_A)
         for j in range(m):
             att[j, :, h * V_A:(h + 1) * V_A] = res_a[j * own:(j + 1) * own]
+    weights_on(gup, up_s, up_r, 4)
+    copy(wo_a, goa.at[1], oa_s.at[1], oa_r.at[1], s, t ^ 2).wait_recv()
+    send(goa.at[1], goa.at[2], oa_s.at[2], oa_r.at[2], s, t ^ 1)
+    copy(wo_b, gob.at[1], ob_s.at[1], ob_r.at[1], s, t ^ 2).wait_recv()
+    send(gob.at[1], gob.at[2], ob_s.at[2], ob_r.at[2], s, t ^ 1)
     for h in range(heads_b):
         res_b = attend(q_b, key_b, val_b, h, depth_b, V_B)
         for j in range(m):
             att[j, :, start_b + h * V_B:start_b + (h + 1) * V_B] = res_b[j * own:(j + 1) * own]
     for k in range(1, m):
         send(att.at[t ^ k], rows.at[k], at_s.at[k], at_r.at[k], s, t ^ k)
-
-    for k in range(2, n, 2):
-        copy(gup.at[k], gup.at[k], up_s.at[k], up_r.at[k], s ^ k, t).wait_recv()
-        send(gup.at[k], gup.at[k + 1], up_s.at[k + 1], up_r.at[k + 1], s ^ 1, t)
 
     mixed = (jnp.dot(att[t, :, 0:width_a], wo_a[...], preferred_element_type=F32)
              + jnp.dot(att[t, :, start_b:], wo_b[...], preferred_element_type=F32))
@@ -206,6 +228,8 @@
 
     for code in (2, 4, 1):
         xsend(0, code, code)
+    for k in range(6, n, 2):
+        weights_on(gup, up_s, up_r, k)
     xcopy(0, 2, 2).wait_recv()
     xcopy(0, 4, 4).wait_recv()
     diag = copy(
@@ -217,9 +241,7 @@
     xsend(4, 5, 1)
     diag.wait_recv()
     xsend(6, 7, 1)
-    for k in range(2, n, 2):
-        copy(gdown.at[k], gdown.at[k], dn_s.at[k], dn_r.at[k], s ^ k, t).wait_recv()
-        send(gdown.at[k], gdown.at[k + 1], dn_s.at[k + 1], dn_r.at[k + 1], s ^ 1, t)
+    weights_on(gdown, dn_s, dn_r, 2)
     for k in (1, 3, 5, 7):
         xcopy(k - 1, k, 1).wait_recv()
 
@@ -228,56 +250,102 @@
 
     held = halves(s)
     hid[...] = jnp.dot(x[:, columns(0, wrows)], w_up[:, held], preferred_element_type=F32)
-    for k in [1] + list(range(3, n, 2)):
-        copy(gup.at[k], gup.at[k], up_s.at[k], up_r.at[k], s ^ 1, t).wait_recv()
-
-    def up(k, carry):
+
+    def up(k):
         hid[...] += jnp.dot(x[:, columns(k, wrows)], gup[k], preferred_element_type=F32)
+
+    def up_loop(i, carry):
+        k = 2 * i
+        copy(gup.at[k + 1], gup.at[k + 1], up_s.at[k + 1], up_r.at[k + 1], s ^ 1, t).wait_recv()
+        up(k)
+        up(k + 1)
         return carry
 
-    lax.fori_loop(1, n, up, 0)
+    copy(gup.at[1], gup.at[1], up_s.at[1], up_r.at[1], s ^ 1, t).wait_recv()
+    up(1)
+    lax.fori_loop(1, 3, up_loop, 0)
+    weights_on(gdown, dn_s, dn_r, 4)
+    lax.fori_loop(3, n // 2, up_loop, 0)
     act[...] = jnp.square(jnp.maximum(hid[...], 0.0)).astype(BF16)
-    for k in [1] + list(range(3, n, 2)):
-        copy(gdown.at[k], gdown.at[k], dn_s.at[k], dn_r.at[k], s ^ 1, t).wait_recv()
-
-    def split(k, piece):
-        at = columns(k, wcols)
+
+    group = n // 2
+
+    def split(g, k, piece):
+        at = pl.ds(pl.multiple_of(((s ^ k) % group) * wcols, 128), wcols)
         for i in range(4):
-            even[i, :, at] = piece[2 * i * own:(2 * i + 1) * own]
-            odd[i, :, at] = piece[(2 * i + 1) * own:(2 * i + 2) * own].astype(BF16)
-
-    split(0, jnp.dot(act[...], w_down[held, :], preferred_element_type=F32))
-
-    def down(k, carry):
-        split(k, jnp.dot(act[...], gdown[k], preferred_element_type=F32))
-        return carry
-
-    lax.fori_loop(1, n, down, 0)
-
-    first = copy(odd, sib, rs_s.at[0], rs_r.at[0], s, t ^ 1)
-    first.start()
-    pending.append(first)
-    first.wait_recv()
-    mid[...] = (even[3] + sib[3].astype(F32)).astype(BF16)
-    second = copy(mid, land.at[0], rs_s.at[1], rs_r.at[1], s ^ (2 - 2 * core), t ^ (2 * core))
-    second.start()
-    pending.append(second)
-    for i in range(3):
-        even[i] += sib[i].astype(F32)
-    second.wait_recv()
-    even[1 + core] += land[0].astype(F32)
-    for i in (1, 2):
-        part[i - 1] = even[i].astype(BF16)
-    third = copy(part.at[0], land.at[1], rs_s.at[2], rs_r.at[2], s, t ^ 2)
-    third.start()
-    fourth = copy(part.at[1], land.at[2], rs_s.at[3], rs_r.at[3], s ^ 2, t)
-    fourth.start()
-    pending.append(third)
-    pending.append(fourth)
-    third.wait_recv()
-    fourth.wait_recv()
-    summed = even[0] + land[1].astype(F32) + land[2].astype(F32)
-    out[...] = (res[...].astype(F32) + summed).astype(BF16)
+            even[g, i, :, at] = piece[2 * i * own:(2 * i + 1) * own]
+            odd[g, i, :, at] = piece[(2 * i + 1) * own:(2 * i + 2) * own].astype(BF16)
+
+    def down(g, k):
+        split(g, k, jnp.dot(act[...], gdown[k], preferred_element_type=F32))
+
+    def down_loop(g):
+        def step(i, carry):
+            k = 2 * i
+            down(g, k)
+            copy(gdown.at[k + 1], gdown.at[k + 1], dn_s.at[k + 1], dn_r.at[k + 1],
+                 s ^ 1, t).wait_recv()
+            down(g, k + 1)
+            return carry
+        return step
+
+    def first(g):
+        return copy(odd.at[g], sib.at[g], rs_s.at[4 * g], rs_r.at[4 * g], s, t ^ 1)
+
+    def second(g):
+        return copy(mid.at[g], land.at[g, 0], rs_s.at[4 * g + 1], rs_r.at[4 * g + 1],
+                    s ^ (2 - 2 * core), t ^ (2 * core))
+
+    def third(g):
+        return copy(part.at[g, 0], land.at[g, 1], rs_s.at[4 * g + 2], rs_r.at[4 * g + 2],
+                    s, t ^ 2)
+
+    def fourth(g):
+        return copy(part.at[g, 1], land.at[g, 2], rs_s.at[4 * g + 3], rs_r.at[4 * g + 3],
+                    s ^ 2, t)
+
+    def begin(c):
+        c.start()
+        pending.append(c)
+
+    def diagonal(g):
+        first(g).wait_recv()
+        mid[g] = (even[g, 3] + sib[g, 3].astype(F32)).astype(BF16)
+        begin(second(g))
+        for i in range(3):
+            even[g, i] += sib[g, i].astype(F32)
+
+    def straight(g):
+        second(g).wait_recv()
+        even[g, 1 + core] += land[g, 0].astype(F32)
+        for i in (1, 2):
+            part[g, i - 1] = even[g, i].astype(BF16)
+        begin(third(g))
+        begin(fourth(g))
+
+    def finish(g):
+        third(g).wait_recv()
+        fourth(g).wait_recv()
+        summed = even[g, 0] + land[g, 1].astype(F32) + land[g, 2].astype(F32)
+        base = (s // group) if g == 0 else 1 - s // group
+        at = pl.ds(pl.multiple_of(base * (group * wcols), 128), group * wcols)
+        out[:, at] = (res[:, at].astype(F32) + summed).astype(BF16)
+
+    split(0, 0, jnp.dot(act[...], w_down[held, :], preferred_element_type=F32))
+    copy(gdown.at[1], gdown.at[1], dn_s.at[1], dn_r.at[1], s ^ 1, t).wait_recv()
+    down(0, 1)
+    for k in range(6, n, 2):
+        weights_on(gdown, dn_s, dn_r, k)
+    lax.fori_loop(1, group // 2, down_loop(0), 0)
+    begin(first(0))
+    diagonal(0)
+    lax.fori_loop(group // 2, n // 2, down_loop(1), 0)
+    straight(0)
+    begin(first(1))
+    diagonal(1)
+    finish(0)
+    straight(1)
+    finish(1)
     for c in pending:
         c.wait_send()
 
@@ -290,10 +358,10 @@
     tail = rotary_key.reshape(lanes, length // lanes, ROPE).transpose(1, 0, 2)
     packed = jnp.concatenate([latent, tail.reshape(length // lanes, rank)], axis=0)
     half = ROPE // 2
-    freqs = THETA ** (-jnp.arange(half, dtype=F32) / half)
-    angle = jnp.arange(n * length, dtype=jnp.int32).astype(F32)[:, None] * freqs
-    cosine, sine = jnp.cos(angle), jnp.sin(angle)
-    table = jnp.concatenate([cosine, cosine, -sine, sine], axis=-1).reshape(n, length, 2 * ROPE)
+    freqs = np.float32(THETA) ** (-np.arange(half, dtype=np.float32) / np.float32(half))
+    angle = np.arange(n * length).astype(np.float32)[:, None] * freqs
+    cosine, sine = np.cos(angle), np.sin(angle)
+    table = jnp.asarray(np.concatenate([cosine, sine], axis=-1).reshape(n, length, ROPE))
     total = n * length
     heads_a = w_key_a.shape[1] // NOPE_A
     heads_b = w_key_b.shape[1] // NOPE_B
@@ -319,14 +387,14 @@
         V((tokens, hidden), F32),
         V((tokens, hidden), BF16),
         V((own, features), BF16),
-        V((m, own, features), F32),
-        V((m, own, features), BF16),
-        V((m, own, features), BF16),
-        V((own, features), BF16),
-        V((2, own, features), BF16),
-        V((3, own, features), BF16),
+        V((2, 4, own, features // 2), F32),
+        V((2, 4, own, features // 2), BF16),
+        V((2, 4, own, features // 2), BF16),
+        V((2, own, features // 2), BF16),
+        V((2, 2, own, features // 2), BF16),
+        V((2, 3, own, features // 2), BF16),
     ]
-    sizes = [n, n, n, n, 3, 3, 3, 3, n, n, n, n, m, m, 8, 8, 4, 4]
+    sizes = [n, n, n, n, 3, 3, 3, 3, n, n, n, n, m, m, 8, 8, 8, 8]
     scratch += [dma(k) for k in sizes]
     return pl.pallas_call(
         functools.partial(kernel, n, m),
@@ -337,8 +405,8 @@
         compiler_params=pltpu.CompilerParams(
             collective_id=0, has_side_effects=True, vmem_limit_bytes=67043328),
         name="layer",
-    )(stream, query_a, query_b, packed, table, latent_gain[None], key_gain_a[None],
-      key_gain_b[None], w_key_a, w_value_a, w_key_b, w_value_b, w_out_a, w_out_b,
+    )(stream, query_a.T, query_b.T, packed, table, latent_gain[None], key_gain_a[None],
+      key_gain_b[None], w_key_a.T, w_value_a.T, w_key_b, w_value_b, w_out_a, w_out_b,
       norm_gain[None], w_up, w_down)
 
 

time: 119 us -> 94.1 us (0.79)
  Pallas kernels: 106 us -> 90.4 us
  other arithmetic: 6.26 us -> 0.67 us
  local copies, waits for them, and re-layouts: 5.84 us -> 2.77 us
    pallas_call x1, Pallas kernels: 106 us -> 90.4 us  [body(): pl.pallas_call(functools.partial(kernel, n, m), out_shape=jax.ShapeDtypeS...]
    unnamed x17 -> x3, local copies, waits for them, and re-layouts: 5.51 us -> 1.67 us
    cos x1 -> x0, other arithmetic: 3.72 us -> none  [body(): cosine, sine = (jnp.cos(angle), jnp.sin(angle))]
    concatenate x1 -> x0, other arithmetic: 1.85 us -> none  [body(): jnp.concatenate([cosine, cosine, -sine, sine], axis=-1)]
where the time goes in v2:
time: 94.1 us; the launch traced here: 93.9 us
  Pallas kernels  90.4 us (96%)
  local copies, waits for them, and re-layouts  2.77 us (3%)
    pallas_call x1, Pallas kernels, body(): pl.pallas_call(functools.partial(kernel, n, m), out_shape=jax.ShapeDtypeS...  90.4 us

profile of v2, /device:TPU:0, one launch (start us, length us, event | category | flops | bytes accessed | tf_op | source)
XLA Modules:
  0.0 93.9 jit_solution(16197221550612938875)
XLA Ops:
  0.0 0.0 copy-start
  0.0 0.9 reshape.6
  0.9 0.1 copy.19
  1.0 0.1 reshape.7
  1.1 0.0 copy-done
  1.1 0.7 pad_maximum_fusion.packed
  1.8 90.4 %layer.1 = bf16[64,2048]{1,0:T(8,128)(2,1)} custom-call(bf16[64,2048]{1,0:T(8,128)(2,1)} %stream.1, bf16[96,256]{1,0:T(8,128)(2,1)} %bitcast.13, bf16[160,256]{1,0:T(8,128)(2,1)} %bitcast.12, bf16[288,256]{1,0:T(8,128)(2,1)} %pad_maximum_fusion.packed, f32[8,256,32]{2,1,0:T(8,128)} %constant.2.clone.table, f32[1,256]{1,0:T(1,128)} %bitcast.17, ...), custom_call_target="tpu_custom_call" | custom-call | tf_op jit(solution)/shard_map/layer/pallas_call | solution.py:399
  92.2 1.7 %copy.21 = bf16[64,2048]{1,0:T(8,128)(2,1)} copy(bf16[64,2048]{1,0:T(8,128)(2,1)} %layer.1) | data formatting | bytes 524288
Async XLA Ops:
  0.0 1.1 %copy-start = (bf16[256,256]{1,0:T(8,128)(2,1)S(1)}, bf16[256,256]{1,0:T(8,128)(2,1)}, u32[]{:S(2)}) copy-start(bf16[256,256]{1,0:T(8,128)(2,1)} %param.21) | copy-start | bytes 393220

commit v3 on v2

--- a/solution.py
+++ b/solution.py
@@ -150,6 +150,7 @@
 
     lax.fori_loop(1, n, one, 0)
     weights_on(gup, up_s, up_r, 2)
+    weights_on(gup, up_s, up_r, 4)
 
     total = n * length
     block = min(total, 2048)
@@ -184,7 +185,6 @@
         res_a = attend(q_a, key_a, val_a, h, depth_a, V_A)
         for j in range(m):
             att[j, :, h * V_A:(h + 1) * V_A] = res_a[j * own:(j + 1) * own]
-    weights_on(gup, up_s, up_r, 4)
     copy(wo_a, goa.at[1], oa_s.at[1], oa_r.at[1], s, t ^ 2).wait_recv()
     send(goa.at[1], goa.at[2], oa_s.at[2], oa_r.at[2], s, t ^ 1)
     copy(wo_b, gob.at[1], ob_s.at[1], ob_r.at[1], s, t ^ 2).wait_recv()
@@ -230,6 +230,7 @@
         xsend(0, code, code)
     for k in range(6, n, 2):
         weights_on(gup, up_s, up_r, k)
+    weights_on(gdown, dn_s, dn_r, 2)
     xcopy(0, 2, 2).wait_recv()
     xcopy(0, 4, 4).wait_recv()
     diag = copy(
@@ -241,7 +242,7 @@
     xsend(4, 5, 1)
     diag.wait_recv()
     xsend(6, 7, 1)
-    weights_on(gdown, dn_s, dn_r, 2)
+    weights_on(gdown, dn_s, dn_r, 4)
     for k in (1, 3, 5, 7):
         xcopy(k - 1, k, 1).wait_recv()
 
@@ -264,8 +265,9 @@
     copy(gup.at[1], gup.at[1], up_s.at[1], up_r.at[1], s ^ 1, t).wait_recv()
     up(1)
     lax.fori_loop(1, 3, up_loop, 0)
-    weights_on(gdown, dn_s, dn_r, 4)
     lax.fori_loop(3, n // 2, up_loop, 0)
+    for k in range(6, n, 2):
+        weights_on(gdown, dn_s, dn_r, k)
     act[...] = jnp.square(jnp.maximum(hid[...], 0.0)).astype(BF16)
 
     group = n // 2
@@ -334,8 +336,6 @@
     split(0, 0, jnp.dot(act[...], w_down[held, :], preferred_element_type=F32))
     copy(gdown.at[1], gdown.at[1], dn_s.at[1], dn_r.at[1], s ^ 1, t).wait_recv()
     down(0, 1)
-    for k in range(6, n, 2):
-        weights_on(gdown, dn_s, dn_r, k)
     lax.fori_loop(1, group // 2, down_loop(0), 0)
     begin(first(0))
     diagonal(0)

time: 94.1 us -> 88.6 us (0.942)
  Pallas kernels: 90.4 us -> 84.9 us
    pallas_call x1, Pallas kernels: 90.4 us -> 84.9 us  [body(): pl.pallas_call(functools.partial(kernel, n, m), out_shape=jax.ShapeDtypeS...]
where the time goes in v3:
time: 88.6 us; the launch traced here: 88.4 us
  Pallas kernels  84.9 us (96%)
  local copies, waits for them, and re-layouts  2.77 us (3%)
    pallas_call x1, Pallas kernels, body(): pl.pallas_call(functools.partial(kernel, n, m), out_shape=jax.ShapeDtypeS...  84.9 us

profile of v3, /device:TPU:0, one launch (start us, length us, event | category | flops | bytes accessed | tf_op | source)
XLA Modules:
  0.0 88.4 jit_solution(14321895806806933897)
XLA Ops:
  0.0 0.0 copy-start
  0.0 0.9 reshape.6
  0.9 0.1 copy.19
  1.0 0.1 reshape.7
  1.1 0.0 copy-done
  1.1 0.7 pad_maximum_fusion.packed
  1.8 84.9 %layer.1 = bf16[64,2048]{1,0:T(8,128)(2,1)} custom-call(bf16[64,2048]{1,0:T(8,128)(2,1)} %stream.1, bf16[96,256]{1,0:T(8,128)(2,1)} %bitcast.13, bf16[160,256]{1,0:T(8,128)(2,1)} %bitcast.12, bf16[288,256]{1,0:T(8,128)(2,1)} %pad_maximum_fusion.packed, f32[8,256,32]{2,1,0:T(8,128)} %constant.2.clone.table, f32[1,256]{1,0:T(1,128)} %bitcast.17, ...), custom_call_target="tpu_custom_call" | custom-call | tf_op jit(solution)/shard_map/layer/pallas_call | solution.py:399
  86.7 1.7 %copy.21 = bf16[64,2048]{1,0:T(8,128)(2,1)} copy(bf16[64,2048]{1,0:T(8,128)(2,1)} %layer.1) | data formatting | bytes 524288
Async XLA Ops:
  0.0 1.1 %copy-start = (bf16[256,256]{1,0:T(8,128)(2,1)S(1)}, bf16[256,256]{1,0:T(8,128)(2,1)}, u32[]{:S(2)}) copy-start(bf16[256,256]{1,0:T(8,128)(2,1)} %param.21) | copy-start | bytes 393220
